TPU v7x, 256 devices: a 4x2x16 block of a 4x16x16 slice. The times are simulated.
256 devices in a mesh: grp: 2 (over y), sp: 32 (over z, core), tp: 4 (over x).
Axes of the slice: x: 4, y: 2, z: 16, core: 2. Of those that a mesh axis runs over, the one named last changes fastest.
The devices are a block of a 4x16x16 slice.
Arguments:
- query_plain: bfloat16 [10240, 1024], P(('grp', 'sp'), 'tp'), parts along dimension 0, may hold values from -6 to 6
- query_turn: bfloat16 [10240, 512], P(('grp', 'sp'), 'tp'), parts along dimension 0, may hold values from -40 to 40, as said below
- latent: bfloat16 [10240, 512], P(('grp', 'sp')), parts along dimension 0, may hold values from -6 to 6
- key_turn: bfloat16 [10240, 64], P(('grp', 'sp')), parts along dimension 0, may hold values from -40 to 40, as said below
- latent_norm_scale: bfloat16 [512], replicated, may hold values from 0.099609375 to 1.8984375
- plain_key_matrix: bfloat16 [512, 1024], P(None, 'tp'), may hold values from -0.25 to 0.25
- value_matrix: bfloat16 [512, 1024], P(None, 'tp'), may hold values from -0.25 to 0.25
- residual: bfloat16 [10240, 2048], P(('grp', 'sp', 'tp')), parts along dimension 0, may hold values from -6 to 6
- out_weight: bfloat16 [1024, 2048], replicated, may hold values from -6 to 6
- ffn_gain: bfloat16 [2048], replicated, may hold values from 0.099609375 to 1.8984375
- gate_weight: bfloat16 [32, 2048, 1024], P('sp', None, 'tp'), may hold values from -1 to 1
- up_weight: bfloat16 [32, 2048, 1024], P('sp', None, 'tp'), may hold values from -1 to 1
- down_weight: bfloat16 [32, 1024, 2048], P('sp', 'tp'), may hold values from -0.0625 to 0.0625
- routes: int32 [10240, 4], P(('grp', 'sp', 'tp')), parts along dimension 0, may hold values from 0 to 31, all different within a row; in each aligned block of 40 rows (0 to 39, 40 to 79, ...) at most 7 rows name the same one
- route_weights: float32 [10240, 4], P(('grp', 'sp', 'tp')), parts along dimension 0, may hold values from 0.1 to 0.6
Outputs:
- mixed: bfloat16 [10240, 2048], P(('grp', 'sp', 'tp')), parts along dimension 0
There are 2 independent parts, one for each index of `grp`. A program takes and returns all parts, laid end to end along the dimension named above; an argument that names none is the same for every part. Nothing has to cross between parts.
Inputs may be any that keep to these rules, and one draw needn't show every extreme that they name: `query_turn`: in the hidden draw some rows are large. `key_turn`: in the hidden draw some rows are large. `routes`: each row names 4 different experts. In each aligned block of 40 rows (the rows of one device) no expert is named more than 7 times, a bound that some block reaches.
All inputs are finite; a program needn't handle non-finite values.
Results may differ from a plain program's by a relative error of at most 0.015.
Values may be sent and summed in bfloat16 or wider, within the bound.
No kernel may reach another device: no remote copies, remote signals or barrier semaphores. Data moves between devices by JAX's collectives and lax.ppermute only.
A program may use at most 128 MiB of HBM per device.

v0:
```python
import jax
import jax.numpy as jnp
from jax import lax
from jax.sharding import Mesh
from jax.sharding import PartitionSpec as P

PLAIN_HEAD_WIDTH = 128
QK_ROPE = 64
VALUE_WIDTH = 128
GRID_W = 64
SP = ("sp_0", "sp_1")
GRP_SP = ("grp", "sp_0", "sp_1")
GRP_SP_TP = ("grp", "sp_0", "sp_1", "tp")
theta = 10000.0
eps = 1e-06
limit = 7.0
slope = 1.702


def sent_together(arrays, axis, dim, along):
    both = jnp.concatenate(arrays, axis=along)
    result, at, finished = (lax.all_gather(both, axis, axis=dim, tiled=True), 0, [])
    for a in arrays:
        finished.append(lax.slice_in_dim(result, at, at + a.shape[along], axis=along))
        at += a.shape[along]
    return tuple(finished)


def turned_gather(arrays, axis, dims):
    turned = [jnp.moveaxis(a, dim, 0) for a, dim in zip(arrays, dims)]
    both = jnp.concatenate([t.reshape(len(t), -1) for t in turned], axis=1)
    result, at, finished = (lax.all_gather(both, axis, axis=0, tiled=True), 0, [])
    for t, dim in zip(turned, dims):
        share = result[:, at : at + t[0].size].reshape(-1, *t.shape[1:])
        finished.append(jnp.moveaxis(share, 0, dim))
        at += t[0].size
    return tuple(finished)


def cut_along(array, dim, count):
    lengths = array.shape
    blocks = array.reshape(*lengths[:dim], count, lengths[dim] // count, *lengths[dim + 1 :])
    return jnp.moveaxis(blocks, dim, 0)


def laid_out(blocks, dim):
    lengths = list(blocks.shape[1:])
    lengths[dim] *= blocks.shape[0]
    return jnp.moveaxis(blocks, 0, dim).reshape(lengths)


def moved_by_axis(blocks, axes, order):
    inside = blocks.shape[1:]
    result = blocks.reshape(*(lax.axis_size(a) for a in axes), *inside)
    for k in order:
        result = lax.all_to_all(result, axes[k], k, k, tiled=True)
    return result.reshape(-1, *inside)


def exchange_by_chip(array, groups, order, split_dim, concat_dim):
    count = lax.axis_size(groups[0]) * lax.axis_size(groups[1])
    blocks = cut_along(array, split_dim, count)
    return laid_out(moved_by_axis(blocks, groups, order), concat_dim)


def turn(vector, row_shift, col_shift):
    width = vector.shape[-1]
    count = width // 4
    half = width // 2
    freqs = theta ** (-jnp.arange(count, dtype=jnp.float32) / count)
    extra = (1,) * (vector.ndim - 2)
    pieces = []
    for portion, shift in ((vector[..., :half], row_shift), (vector[..., half:], col_shift)):
        angle = (shift.astype(jnp.float32)[:, None] * freqs[None, :]).reshape(
            (shift.shape[0],) + extra + (count,)
        )
        lower = portion[..., :count]
        upper = portion[..., count:]
        pieces.append(
            jnp.concatenate(
                [
                    lower * jnp.cos(angle) - upper * jnp.sin(angle),
                    lower * jnp.sin(angle) + upper * jnp.cos(angle),
                ],
                axis=-1,
            )
        )
    return jnp.concatenate(pieces, axis=-1)


def norm_scale(values, gain):
    wide = values.astype(jnp.float32)
    return (
        wide
        * lax.rsqrt(jnp.mean(wide * wide, axis=-1, keepdims=True) + eps)
        * gain.astype(jnp.float32)
    )


def expert_active(rows, gate_w, up_w):
    gate_pre = jnp.minimum(jnp.dot(rows, gate_w, preferred_element_type=jnp.float32), limit)
    up_pre = jnp.clip(jnp.dot(rows, up_w, preferred_element_type=jnp.float32), -limit, limit)
    return ((up_pre + 1.0) * gate_pre * jax.nn.sigmoid(slope * gate_pre)).astype(jnp.bfloat16)


def expert_whole(rows, gate_w, up_w, down_w, groups):
    active = expert_active(rows, gate_w, up_w)
    piece = down_w.shape[0] // groups
    total = jnp.zeros((rows.shape[0], down_w.shape[1]), jnp.float32)
    for index in range(groups):
        product = jnp.dot(
            active[:, index * piece : (index + 1) * piece],
            down_w[index * piece : (index + 1) * piece],
            preferred_element_type=jnp.float32,
        )
        total = total + product.astype(jnp.bfloat16).astype(jnp.float32)
    return total.astype(jnp.bfloat16)


def on_device(
    query_plain,
    query_turn,
    latent,
    key_turn,
    latent_norm_scale,
    plain_key_matrix,
    value_matrix,
    residual,
    out_weight,
    ffn_gain,
    gate_weight,
    up_weight,
    down_weight,
    routes,
    route_weights,
):
    tok_dev = latent.shape[0]
    heads_dev = query_plain.shape[1] // PLAIN_HEAD_WIDTH
    model_width = residual.shape[1]
    place = lax.axis_index(SP) * tok_dev + jnp.arange(tok_dev, dtype=jnp.int32)
    grid_row = place // GRID_W
    grid_col = place % GRID_W
    normed_latent = norm_scale(latent, latent_norm_scale).astype(jnp.bfloat16)
    key_plain = jnp.dot(normed_latent, plain_key_matrix, preferred_element_type=jnp.float32).astype(
        jnp.bfloat16
    )
    values = jnp.dot(normed_latent, value_matrix, preferred_element_type=jnp.float32).astype(
        jnp.bfloat16
    )
    key_rot = turn(key_turn.astype(jnp.float32), grid_row, grid_col).astype(jnp.bfloat16)
    key_pairs = key_rot.reshape(tok_dev // 2, 2 * QK_ROPE)
    query_rot = turn(
        query_turn.astype(jnp.float32).reshape(tok_dev, heads_dev, QK_ROPE), grid_row, grid_col
    ).astype(jnp.bfloat16)
    plain_query = query_plain.reshape(tok_dev, heads_dev, PLAIN_HEAD_WIDTH)
    scale = (PLAIN_HEAD_WIDTH + QK_ROPE) ** (-0.5)
    most = jnp.full((heads_dev, tok_dev), -jnp.inf, jnp.float32)
    total = jnp.zeros((heads_dev, tok_dev), jnp.float32)
    summed = jnp.zeros((heads_dev, tok_dev, VALUE_WIDTH), jnp.float32)
    piece_keys, piece_values, piece_pairs = (
        *sent_together((key_plain, values), SP, 0, 1),
        lax.all_gather(key_pairs, SP, axis=0, tiled=True),
    )
    count = piece_keys.shape[0]
    piece_rot = piece_pairs.reshape(count, QK_ROPE)
    new_most = []
    new_total = []
    new_summed = []
    for head in range(heads_dev):
        head_keys = piece_keys[:, head * PLAIN_HEAD_WIDTH : (head + 1) * PLAIN_HEAD_WIDTH]
        head_values = piece_values[:, head * VALUE_WIDTH : (head + 1) * VALUE_WIDTH]
        scores = (
            jnp.einsum(
                "qd,kd->qk", plain_query[:, head], head_keys, preferred_element_type=jnp.float32
            )
            + jnp.einsum(
                "qd,kd->qk", query_rot[:, head], piece_rot, preferred_element_type=jnp.float32
            )
        ) * scale
        peak = jnp.max(scores, axis=1)
        factor = jnp.exp(most[head] - peak)
        weights = jnp.exp(scores - peak[:, None])
        new_total.append(total[head] * factor + jnp.sum(weights, axis=1))
        new_summed.append(
            summed[head] * factor[:, None]
            + jnp.dot(weights.astype(jnp.bfloat16), head_values, preferred_element_type=jnp.float32)
        )
        new_most.append(peak)
    total = jnp.stack(new_total)
    summed = jnp.stack(new_summed)
    attended = jnp.transpose((summed / total[..., None]).astype(jnp.bfloat16), (1, 0, 2)).reshape(
        tok_dev, heads_dev * VALUE_WIDTH
    )
    rows_dev = residual.shape[0]
    token_heads = lax.all_to_all(attended, "tp", split_axis=0, concat_axis=1, tiled=True)
    projected = jnp.dot(token_heads, out_weight, preferred_element_type=jnp.float32)
    hidden = (residual.astype(jnp.float32) + projected).astype(jnp.bfloat16)
    normed = norm_scale(hidden, ffn_gain).astype(jnp.bfloat16)
    top_count = routes.shape[1]
    experts_all = lax.axis_size(SP) * gate_weight.shape[0]
    capacity = min(rows_dev, max(2, rows_dev * top_count * 3 // (2 * experts_all)))
    flat_routes = routes.reshape(rows_dev * top_count)
    marks = (flat_routes[:, None] == jnp.arange(experts_all, dtype=jnp.int32)[None, :]).astype(
        jnp.int32
    )
    earlier = jnp.cumsum(marks, axis=0, dtype=jnp.int32) - marks
    slots = jnp.sum(earlier * marks, axis=1, dtype=jnp.int32)
    target = flat_routes * capacity + slots
    chosen = (
        target.reshape(rows_dev, top_count)[None, :, :]
        == jnp.arange(experts_all * capacity, dtype=jnp.int32)[:, None, None]
    )
    dispatch_table = jnp.sum(chosen.astype(jnp.bfloat16), axis=2)
    outgoing = jnp.dot(dispatch_table, normed, preferred_element_type=jnp.float32).astype(
        jnp.bfloat16
    )
    outgoing = outgoing.reshape(experts_all, capacity, model_width)
    gate_w = gate_weight[0]
    up_w = up_weight[0]
    down_w = down_weight[0]
    group = lax.axis_size("tp")
    gate_full, up_full, down_full = turned_gather((gate_w, up_w, down_w), "tp", (1, 1, 0))
    arrived = lax.all_to_all(outgoing, SP, split_axis=0, concat_axis=0, tiled=True)
    result_rows = expert_whole(
        arrived.reshape(experts_all * capacity, model_width), gate_full, up_full, down_full, group
    )
    returned = exchange_by_chip(
        result_rows.reshape(experts_all, capacity, model_width), ("sp_0", "sp_1"), (1, 0), 0, 0
    )
    picked = returned.reshape(experts_all * capacity, model_width)[target]
    picked = picked.reshape(rows_dev, top_count, model_width).astype(jnp.float32)
    return (hidden.astype(jnp.float32) + jnp.sum(route_weights[..., None] * picked, axis=1)).astype(
        jnp.bfloat16
    )


def solution(mesh):
    torus = Mesh(
        mesh.devices.reshape(mesh.shape["grp"], 16, 2, mesh.shape["tp"]),
        ("grp", "sp_0", "sp_1", "tp"),
    )
    placed = (
        P(GRP_SP, "tp"),
        P(GRP_SP, "tp"),
        P(GRP_SP, None),
        P(GRP_SP, None),
        P(),
        P(None, "tp"),
        P(None, "tp"),
        P(GRP_SP_TP, None),
        P(),
        P(),
        P(SP, None, "tp"),
        P(SP, None, "tp"),
        P(SP, "tp", None),
        P(GRP_SP_TP, None),
        P(GRP_SP_TP, None),
    )
    return jax.shard_map(
        on_device, mesh=torus, in_specs=placed, out_specs=P(GRP_SP_TP, None), check_vma=False
    )
```

profile of v0, /device:TPU:34, one launch (start us, length us, event | category | flops | bytes accessed | tf_op | source)
XLA Modules:
  0.0 310.7 jit_solution(7776849853484320127)
XLA Ops:
  6.6 0.8 convert_element_type.119
  7.3 1.0 fusion.74
  8.4 1.2 convolution_convert_fusion.5
  9.6 1.3 convolution_convert_fusion.6
  10.8 0.7 pad_maximum_fusion.1
  11.7 1.5 copy.71
  13.2 0.6 copy.70
  13.8 2.8 pad_maximum_fusion
  16.8 0.2 multiply_cosine_fusion.1
  17.0 0.1 copy.61
  17.2 0.1 convert_element_type.126
  17.3 52.1 %all_gather.10 = bf16[2560,128]{1,0:T(8,128)(2,1)S(1)} all-gather(bf16[80,128]{1,0:T(8,128)(2,1)S(1)} %convert_element_type.126), channel_id=1, replica_groups=mesh['grp'=2,'sp_0'=16,'sp_1'=2,'tp'=4] {'sp_0','sp_1'}, dimensions={0}, use_global_device_ids=true | all-gather | bytes 675840 | tf_op jit(solution)/shard_map/all_gather | solution.py:162
  69.3 0.5 reshape.301
  69.9 0.1 copy.60
  70.0 0.1 copy.65
  70.1 0.1 eq.37
  70.3 0.6 reduce-window.6
  70.9 0.2 slice_reduce_fusion
  71.1 0.1 bitcast_bitcast_fusion
  71.2 0.1 reduce_sum.74
  71.3 0.6 broadcast_multiply_fusion
  71.9 0.1 copy.69
  72.1 0.7 fusion.103
  72.8 2.3 fusion.95
  75.1 2.0 fusion.96
  77.1 22.1 %all-gather.3.cloned.1.call-done = bf16[5120,512]{1,0:T(8,128)(2,1)} async-done(((bf16[160,512]{1,0:T(8,128)(2,1)}), bf16[5120,512]{1,0:T(8,128)(2,1)}) %all-gather.3.cloned.1.call-update) | async-done | bytes 5242896 | tf_op jit(solution)/shard_map/all_gather | solution.py:22
  99.2 3.2 %fusion.104 = (f32[160]{0:T(256)S(1)}, f32[160,5120]{1,0:T(8,128)S(1)}) fusion(f32[160,5120]{1,0:T(8,128)} %fusion.95, bf16[160,1,128]{2,1,0:T(2,128)(2,1)S(1)} %copy-done.4, bf16[5120,512]{1,0:T(8,128)(2,1)} %all-gather.3.cloned.1.call-done), kind=kOutput, calls=%fused_computation.135 | convolution fusion | flops 212172640 | bytes 7905920 | tf_op jit(solution)/shard_map/qd,kd->qk/dot_general | solution.py:173
  102.4 0.6 fusion.10
  103.0 0.1 slice-done.1
  103.1 0.7 fusion.105
  103.7 0.6 fusion.8
  104.4 0.7 fusion.65
  105.1 0.7 fusion.55
  105.9 0.1 fusion.86
  106.1 0.7 all_to_all.23
  106.8 4.8 %all-to-all-start = ((bf16[4,40,256]{2,1,0:T(8,128)(2,1)}), bf16[4,40,256]{2,1,0:T(8,128)(2,1)S(1)}, u32[]{:S(2)}, u32[]{:S(2)}) async-start(bf16[4,40,256]{2,1,0:T(8,128)(2,1)} %all_to_all.23), calls=%async_computation | async-start | bytes 163840 | tf_op jit(solution)/shard_map/all_to_all | solution.py:195
  111.5 0.1 fusion.85
  111.6 4.2 %all-to-all-done = bf16[4,40,256]{2,1,0:T(8,128)(2,1)S(1)} async-done(((bf16[4,40,256]{2,1,0:T(8,128)(2,1)}), bf16[4,40,256]{2,1,0:T(8,128)(2,1)S(1)}, u32[]{:S(2)}, u32[]{:S(2)}) %all-to-all-start) | async-done | bytes 81952 | tf_op jit(solution)/shard_map/all_to_all | solution.py:195
  115.8 3.6 %multiply_reduce_fusion.1 = (f32[40]{0:T(128)S(1)}, f32[40,2048]{1,0:T(8,128)S(1)}) fusion(bf16[40,1024]{1,0:T(8,128)(2,1)S(1)} %bitcast.79, bf16[1024,2048]{1,0:T(8,128)(2,1)} %param.23, bf16[40,2048]{1,0:T(8,128)(2,1)S(1)} %copy-done.5), kind=kOutput, calls=%fused_computation.66 | convolution fusion | flops 168263648 | bytes 4767904 | tf_op jit(solution)/shard_map/dot_general | solution.py:196
  119.4 0.5 convolution_convert_fusion.4
  119.9 0.3 reshape.304
  120.2 63.2 %all_to_all.34 = bf16[32,7,2048]{2,1,0:T(8,128)(2,1)S(1)} all-to-all(bf16[32,7,2048]{2,1,0:T(8,128)(2,1)S(1)} %reshape.304), channel_id=1, replica_groups=mesh['grp'=2,'sp_0'=16,'sp_1'=2,'tp'=4] {'sp_0','sp_1'}, dimensions={0} | all-to-all | bytes 1835008 | tf_op jit(solution)/shard_map/all_to_all | solution.py:223
  183.3 0.3 reshape.305
  183.7 38.2 %all-gather.5.cloned.1.call-done = bf16[1024,6144]{1,0:T(8,128)(2,1)} async-done(((bf16[256,6144]{1,0:T(8,128)(2,1)}), bf16[1024,6144]{1,0:T(8,128)(2,1)}) %all-gather.5.cloned.1.call-update) | async-done | bytes 12582928 | tf_op jit(solution)/shard_map/all_gather | solution.py:32
  221.9 3.6 %fusion.44 = f32[224,1024]{1,0:T(8,128)S(1)} fusion(bf16[224,2048]{1,0:T(8,128)(2,1)S(1)} %reshape.305, bf16[1024,6144]{1,0:T(8,128)(2,1)} %all-gather.5.cloned.1.call-done), kind=kOutput, calls=%fused_computation.47 | convolution fusion | flops 939753472 | bytes 6029312 | tf_op jit(solution)/shard_map/dot_general | solution.py:101
  225.5 3.7 %fusion.47 = bf16[224,1024]{1,0:T(8,128)(2,1)S(1)} fusion(f32[224,1024]{1,0:T(8,128)S(1)} %fusion.44, bf16[224,2048]{1,0:T(8,128)(2,1)S(1)} %reshape.305, bf16[1024,6144]{1,0:T(8,128)(2,1)} %all-gather.5.cloned.1.call-done), kind=kOutput, calls=%fused_computation.48 | convolution fusion | flops 941588480 | bytes 6488064 | tf_op jit(solution)/shard_map/dot_general | solution.py:102
  229.2 1.6 fusion.19
  230.9 1.6 fusion.18
  232.5 1.6 fusion.16
  234.1 1.6 fusion.14
  235.8 0.3 reshape_reshape_reshape.6
  236.1 0.6 copy.72
  236.7 4.5 %all_to_all.35 = bf16[16,2,1,7,2048]{4,0,3,2,1:T(8,128)(2,1)S(1)} all-to-all(bf16[16,2,1,7,2048]{4,0,3,2,1:T(8,128)(2,1)S(1)} %copy.72), channel_id=1, replica_groups=mesh['grp'=2,'sp_0'=16,'sp_1'=2,'tp'=4] {'sp_1'}, dimensions={1} | all-to-all | bytes 1835008 | tf_op jit(solution)/shard_map/all_to_all | solution.py:56
  241.2 1.9 copy.73
  243.1 12.4 %all-to-all-start.3 = ((bf16[16,2,1,7,2048]{4,1,3,2,0:T(2,128)(2,1)}), bf16[16,2,1,7,2048]{4,1,3,2,0:T(2,128)(2,1)S(1)}, u32[]{:S(2)}, u32[]{:S(2)}) async-start(bf16[16,2,1,7,2048]{4,1,3,2,0:T(2,128)(2,1)} %copy.73), calls=%async_computation.3 | async-start | bytes 1835008 | tf_op jit(solution)/shard_map/all_to_all | solution.py:56
  255.5 0.1 mul.284
  255.6 0.1 copy.64
  255.7 44.4 %all-to-all-done.3 = bf16[16,2,1,7,2048]{4,1,3,2,0:T(2,128)(2,1)S(1)} async-done(((bf16[16,2,1,7,2048]{4,1,3,2,0:T(2,128)(2,1)}), bf16[16,2,1,7,2048]{4,1,3,2,0:T(2,128)(2,1)S(1)}, u32[]{:S(2)}, u32[]{:S(2)}) %all-to-all-start.3) | async-done | bytes 917536 | tf_op jit(solution)/shard_map/all_to_all | solution.py:56
  300.1 0.4 copy.74
  300.4 0.3 reshape_reshape_reshape.7
  300.8 1.0 gather_fusion
  301.8 0.4 reshape.309
  302.2 0.9 multiply_reduce_fusion
  303.2 0.7 add_convert_fusion
  (57 shorter events, 0.6 us)
Async XLA Ops:
  6.5 1.8 copy-start
  6.6 6.6 %copy-start.3 = (bf16[1,2048,256]{2,1,0:T(8,128)(2,1)S(1)}, bf16[1,2048,256]{2,1,0:T(8,128)(2,1)}, u32[]{:S(2)}) copy-start(bf16[1,2048,256]{2,1,0:T(8,128)(2,1)} %param.25) | copy-start | bytes 3145732
  6.6 92.6 %all-gather.3.cloned.1.call-start = ((), (), s32[]{:S(2)}) async-start(), calls=%async_computation.4 | async-start | bytes 5406720 | tf_op jit(solution)/shard_map/all_gather | solution.py:22
  11.6 210.3 %all-gather.5.cloned.1.call-start = ((), (), s32[]{:S(2)}) async-start(), calls=%async_computation.5 | async-start | bytes 15728640 | tf_op jit(solution)/shard_map/all_gather | solution.py:32
  13.8 2.9 copy-start.9
  16.7 53.2 %copy-start.8 = (bf16[160,128]{1,0:T(8,128)(2,1)S(1)}, bf16[160,128]{1,0:T(8,128)(2,1)}, u32[]{:S(2)}) copy-start(bf16[160,128]{1,0:T(8,128)(2,1)} %param.16) | copy-start | bytes 122884
  16.7 53.3 %copy-start.7 = (bf16[160,256]{1,0:T(8,128)(2,1)S(1)}, bf16[160,256]{1,0:T(8,128)(2,1)}, u32[]{:S(2)}) copy-start(bf16[160,256]{1,0:T(8,128)(2,1)} %param.15) | copy-start | bytes 245764
  16.7 53.4 %copy-start.11 = (s32[40,4]{0,1:T(4,128)S(1)}, s32[40,4]{0,1:T(4,128)}, u32[]{:S(2)}) copy-start(s32[40,4]{0,1:T(4,128)} %param.28) | copy-start | bytes 1924
  16.7 55.3 %copy-start.10 = (bf16[2048]{0:T(1024)(128)(2,1)S(1)}, bf16[2048]{0:T(1024)(128)(2,1)}, u32[]{:S(2)}) copy-start(bf16[2048]{0:T(1024)(128)(2,1)} %param.24) | copy-start | bytes 12292
  69.8 3.0 copy-start.2
  75.1 24.1 %copy-start.4 = (bf16[160,1,128]{2,1,0:T(2,128)(2,1)S(1)}, bf16[160,1,128]{2,1,0:T(2,128)(2,1)}, u32[]{:S(2)}) copy-start(bf16[160,1,128]{2,1,0:T(2,128)(2,1)} %get-tuple-element.12) | copy-start | bytes 122884
  99.2 3.8 %slice-start = ((s8[5242880]{0:T(1024)(128)(4,1)}), s8[4194304]{0:T(1024)(128)(4,1)S(1)}, s32[]{:S(2)}) async-start(s8[5242880]{0:T(1024)(128)(4,1)} %bitcast.73), calls=%async_computation.6 | async-start | bytes 8388608
  99.2 3.9 %slice-start.1 = ((s8[5242880]{0:T(1024)(128)(4,1)}), s8[1048576]{0:T(1024)(128)(4,1)S(1)}, s32[]{:S(2)}) async-start(s8[5242880]{0:T(1024)(128)(4,1)} %bitcast.73), calls=%async_computation.7 | async-start | bytes 2097152
  105.1 10.7 %copy-start.5 = (bf16[40,2048]{1,0:T(8,128)(2,1)S(1)}, bf16[40,2048]{1,0:T(8,128)(2,1)}, u32[]{:S(2)}) copy-start(bf16[40,2048]{1,0:T(8,128)(2,1)} %param.22) | copy-start | bytes 491524
  106.8 9.0 %all-to-all-start = ((bf16[4,40,256]{2,1,0:T(8,128)(2,1)}), bf16[4,40,256]{2,1,0:T(8,128)(2,1)S(1)}, u32[]{:S(2)}, u32[]{:S(2)}) async-start(bf16[4,40,256]{2,1,0:T(8,128)(2,1)} %all_to_all.23), calls=%async_computation | async-start | bytes 163840 | tf_op jit(solution)/shard_map/all_to_all | solution.py:195
  236.1 19.3 %copy-start.6 = (s32[40,4]{1,0:T(8,128)S(1)}, s32[40,4]{1,0:T(8,128)}, u32[]{:S(2)}) copy-start(s32[40,4]{1,0:T(8,128)} %get-tuple-element.19) | copy-start | bytes 1924
  236.1 19.4 %copy-start.12 = (f32[40,4]{0,1:T(4,128)S(1)}, f32[40,4]{0,1:T(4,128)}, u32[]{:S(2)}) copy-start(f32[40,4]{0,1:T(4,128)} %param.29) | copy-start | bytes 1924
  243.1 57.0 %all-to-all-start.3 = ((bf16[16,2,1,7,2048]{4,1,3,2,0:T(2,128)(2,1)}), bf16[16,2,1,7,2048]{4,1,3,2,0:T(2,128)(2,1)S(1)}, u32[]{:S(2)}, u32[]{:S(2)}) async-start(bf16[16,2,1,7,2048]{4,1,3,2,0:T(2,128)(2,1)} %copy.73), calls=%async_computation.3 | async-start | bytes 1835008 | tf_op jit(solution)/shard_map/all_to_all | solution.py:56
  300.8 3.1 %copy-start.1 = (bf16[512,256]{1,0:T(8,128)(2,1)S(1)}, bf16[512,256]{1,0:T(8,128)(2,1)}, u32[]{:S(2)}) copy-start(bf16[512,256]{1,0:T(8,128)(2,1)} %param.21) | copy-start | bytes 786436
Sparse Core Ops, SparseCore 0:
  11.7 87.4 all-gather.2
  101.0 120.8 all-gather.4
where the time goes:
time: 312 us; the launch traced here: 311 us
  blocking collectives  120 us (38%)
  waiting for transfers between devices  109 us (35%)
  matrix products  29.9 us (10%)
  starting transfers between devices  17.2 us (6%)
  between operations  13.9 us (4%)
  local copies, waits for them, and re-layouts  10.8 us (3%)
  other arithmetic  10.1 us (3%)
    all_to_all x1, blocking collectives, on_device(): lax.all_to_all(outgoing, SP, split_axis=0, concat_axis=0, tiled=True)  63.2 us
    all_gather x1, blocking collectives, on_device(): lax.all_gather(key_pairs, SP, axis=0, tiled=True)  52.1 us
    all_to_all x1, waiting for transfers between devices, moved_by_axis(): result = lax.all_to_all(result, axes[k], k, k, tiled=True)  44.4 us
    all_gather x1, waiting for transfers between devices, turned_gather(): lax.all_gather(both, axis, axis=0, tiled=True)  38.2 us
    all_gather x1, waiting for transfers between devices, sent_together(): lax.all_gather(both, axis, axis=dim, tiled=True)  22.1 us
    all_to_all x1, starting transfers between devices, moved_by_axis(): result = lax.all_to_all(result, axes[k], k, k, tiled=True)  12.4 us
    dot_general x4, matrix products, expert_whole(): jnp.dot(active[:, index * piece:(index + 1) * piece], down_w[index * piec...  6.55 us
  transfers between devices with their start and end apart: 4, of which 4 were waited for; matrix products, arithmetic and copies ran while one was open for 8% of the time, Pallas kernels for 0%

commit v1 on v0

--- a/solution.py
+++ b/solution.py
@@ -29,7 +29,13 @@
 def turned_gather(arrays, axis, dims):
     turned = [jnp.moveaxis(a, dim, 0) for a, dim in zip(arrays, dims)]
     both = jnp.concatenate([t.reshape(len(t), -1) for t in turned], axis=1)
-    result, at, finished = (lax.all_gather(both, axis, axis=0, tiled=True), 0, [])
+    return_all_the_groups = lambda local_x, bus_axis: jnp.concatenate(
+        lax.all_to_all(
+            jnp.stack([local_x] * lax.axis_size(bus_axis), 0), bus_axis, split_axis=0, concat_axis=0
+        ),
+        0,
+    )
+    result, at, finished = (return_all_the_groups(both, axis), 0, [])
     for t, dim in zip(turned, dims):
         share = result[:, at : at + t[0].size].reshape(-1, *t.shape[1:])
         finished.append(jnp.moveaxis(share, 0, dim))

time: 312 us -> 420 us (1.35)
  waiting for transfers between devices: 109 us -> 263 us
  blocking collectives: 120 us -> 55.8 us
  local copies, waits for them, and re-layouts: 10.8 us -> 20.4 us
  starting transfers between devices: 17.2 us -> 25.3 us
    all_to_all x0 -> x2, waiting for transfers between devices: none -> 187 us  [the longest x1 136 us: turned_gather(): lax.all_to_all(jnp.stack([local_x] * lax.axis_size(bus_axis), 0), bus_axi...]
    all_to_all x1 -> x0, blocking collectives: 63.2 us -> none  [on_device(): lax.all_to_all(outgoing, SP, split_axis=0, concat_axis=0, tiled=True)]
    all_gather x1 -> x0, waiting for transfers between devices: 38.2 us -> none  [turned_gather(): lax.all_gather(both, axis, axis=0, tiled=True)]
    all_to_all x0 -> x2, starting transfers between devices: none -> 15.7 us  [the longest x1 7.92 us: turned_gather(): lax.all_to_all(jnp.stack([local_x] * lax.axis_size(bus_axis), 0), bus_axi...]
    all_to_all x1, starting transfers between devices: 12.4 us -> 4.07 us  [moved_by_axis(): result = lax.all_to_all(result, axes[k], k, k, tiled=True)]
    another operation x1 -> x2, local copies, waits for them, and re-layouts: 0.01 us -> 6.04 us  [the longest x1 6.03 us: turned_gather(): jnp.stack([local_x] * lax.axis_size(bus_axis), 0)]
    all_gather x1, waiting for transfers between devices: 22.1 us -> 26.5 us  [sent_together(): lax.all_gather(both, axis, axis=dim, tiled=True)]
  transfers between devices with their start and end apart: 4 -> 5, of which waited for: 4 -> 5; matrix products, arithmetic and copies ran while one was open for 8% -> 4% of each run, Pallas kernels for 0% -> 0%
where the time goes in v1:
time: 420 us; the launch traced here: 418 us
  waiting for transfers between devices  263 us (63%)
  blocking collectives  55.8 us (13%)
  matrix products  29.5 us (7%)
  starting transfers between devices  25.3 us (6%)
  local copies, waits for them, and re-layouts  20.4 us (5%)
  between operations  13.9 us (3%)
  other arithmetic  10 us (2%)
    all_to_all x1, waiting for transfers between devices, turned_gather(): lax.all_to_all(jnp.stack([local_x] * lax.axis_size(bus_axis), 0), bus_axi...  136 us
    all_gather x1, blocking collectives, on_device(): lax.all_gather(key_pairs, SP, axis=0, tiled=True)  51.3 us
    all_to_all x1, waiting for transfers between devices, on_device(): lax.all_to_all(outgoing, SP, split_axis=0, concat_axis=0, tiled=True)  50.5 us
    all_to_all x1, waiting for transfers between devices, moved_by_axis(): result = lax.all_to_all(result, axes[k], k, k, tiled=True)  45.5 us
    all_gather x1, waiting for transfers between devices, sent_together(): lax.all_gather(both, axis, axis=dim, tiled=True)  26.5 us
  transfers between devices with their start and end apart: 5, of which 5 were waited for; matrix products, arithmetic and copies ran while one was open for 4% of the time, Pallas kernels for 0%

profile of v1, /device:TPU:34, one launch (start us, length us, event | category | flops | bytes accessed | tf_op | source)
XLA Modules:
  0.0 418.1 jit_solution(3674537627970618317)
XLA Ops:
  6.6 0.8 convert_element_type.119
  7.4 1.0 fusion.74
  8.5 1.2 convolution_convert_fusion.5
  9.6 1.3 convolution_convert_fusion.6
  10.9 0.7 pad_maximum_fusion.1
  11.7 0.8 convert_element_type.125
  12.4 0.2 multiply_cosine_fusion.1
  12.7 0.1 copy.61
  12.8 0.1 convert_element_type.126
  12.9 51.3 %all_gather.7 = bf16[2560,128]{1,0:T(8,128)(2,1)S(1)} all-gather(bf16[80,128]{1,0:T(8,128)(2,1)S(1)} %convert_element_type.126), channel_id=1, replica_groups=mesh['grp'=2,'sp_0'=16,'sp_1'=2,'tp'=4] {'sp_0','sp_1'}, dimensions={0}, use_global_device_ids=true | all-gather | bytes 675840 | tf_op jit(solution)/shard_map/all_gather | solution.py:168
  64.2 0.5 reshape.306
  64.8 0.1 copy.60
  64.9 0.1 copy.65
  65.0 0.1 eq.37
  65.2 0.6 reduce-window.6
  65.8 0.2 slice_reduce_fusion
  66.1 0.1 reduce_sum.74
  66.2 0.6 broadcast_multiply_fusion
  67.0 0.7 fusion.103
  67.7 2.3 fusion.95
  70.0 2.0 fusion.96
  72.0 26.5 %all-gather.2.cloned.1.call-done = bf16[5120,512]{1,0:T(8,128)(2,1)} async-done(((bf16[160,512]{1,0:T(8,128)(2,1)}), bf16[5120,512]{1,0:T(8,128)(2,1)}) %all-gather.2.cloned.1.call-update) | async-done | bytes 5242896 | tf_op jit(solution)/shard_map/all_gather | solution.py:22
  98.5 3.2 fusion.104
  101.7 0.6 fusion.10
  102.4 0.7 fusion.105
  103.1 0.6 fusion.8
  103.7 0.7 fusion.65
  104.5 0.7 fusion.55
  105.3 0.1 fusion.86
  105.5 0.7 all_to_all.26
  106.1 5.5 %all-to-all-start = ((bf16[4,40,256]{2,1,0:T(8,128)(2,1)}), bf16[4,40,256]{2,1,0:T(8,128)(2,1)S(1)}, u32[]{:S(2)}, u32[]{:S(2)}) async-start(bf16[4,40,256]{2,1,0:T(8,128)(2,1)} %all_to_all.26), calls=%async_computation | async-start | bytes 163840 | tf_op jit(solution)/shard_map/all_to_all | solution.py:201
  111.7 4.2 all-to-all-done
  115.9 3.1 multiply_reduce_fusion.1
  119.1 0.7 copy-done.3
  119.8 0.4 convolution_convert_fusion.4
  120.2 1.3 reshape.309
  121.5 7.8 %all-to-all-start.1 = ((bf16[32,7,2048]{2,1,0:T(8,128)(2,1)}), bf16[32,7,2048]{2,1,0:T(8,128)(2,1)}, u32[]{:S(2)}, u32[]{:S(2)}) async-start(bf16[32,7,2048]{2,1,0:T(8,128)(2,1)} %reshape.309), calls=%async_computation.1 | async-start | bytes 2097152 | tf_op jit(solution)/shard_map/all_to_all | solution.py:229
  129.3 1.4 copy.71
  130.7 1.4 copy.70
  132.1 2.0 pad_maximum_fusion
  134.1 50.5 %all-to-all-done.1 = bf16[32,7,2048]{2,1,0:T(8,128)(2,1)} async-done(((bf16[32,7,2048]{2,1,0:T(8,128)(2,1)}), bf16[32,7,2048]{2,1,0:T(8,128)(2,1)}, u32[]{:S(2)}, u32[]{:S(2)}) %all-to-all-start.1) | async-done | bytes 917536 | tf_op jit(solution)/shard_map/all_to_all | solution.py:229
  184.6 6.0 %stack.25 = bf16[4,256,6144]{2,1,0:T(8,128)(2,1)} broadcast(bf16[256,6144]{1,0:T(8,128)(2,1)S(1)} %pad_maximum_fusion), dimensions={1,2} | broadcast | bytes 15728640 | tf_op jit(solution)/shard_map/stack | solution.py:34
  190.7 7.9 %all-to-all-start.2 = ((bf16[4,256,6144]{2,1,0:T(8,128)(2,1)}), bf16[4,256,6144]{2,1,0:T(8,128)(2,1)}, u32[]{:S(2)}, u32[]{:S(2)}) async-start(bf16[4,256,6144]{2,1,0:T(8,128)(2,1)} %stack.25), calls=%async_computation.2 | async-start | bytes 25165824 | tf_op jit(solution)/shard_map/all_to_all | solution.py:33
  198.6 1.5 reshape.310
  200.1 136.3 %all-to-all-done.2 = bf16[4,256,6144]{2,1,0:T(8,128)(2,1)} async-done(((bf16[4,256,6144]{2,1,0:T(8,128)(2,1)}), bf16[4,256,6144]{2,1,0:T(8,128)(2,1)}, u32[]{:S(2)}, u32[]{:S(2)}) %all-to-all-start.2) | async-done | bytes 12582944 | tf_op jit(solution)/shard_map/all_to_all | solution.py:33
  336.4 3.6 fusion.44
  340.0 3.7 fusion.47
  343.7 1.6 fusion.19
  345.4 1.6 fusion.18
  347.0 1.6 fusion.16
  348.7 1.6 fusion.14
  350.3 0.3 reshape_reshape_reshape.6
  350.6 0.6 copy.72
  351.2 4.5 %all_to_all.39 = bf16[16,2,1,7,2048]{4,0,3,2,1:T(8,128)(2,1)S(1)} all-to-all(bf16[16,2,1,7,2048]{4,0,3,2,1:T(8,128)(2,1)S(1)} %copy.72), channel_id=1, replica_groups=mesh['grp'=2,'sp_0'=16,'sp_1'=2,'tp'=4] {'sp_1'}, dimensions={1} | all-to-all | bytes 1835008 | tf_op jit(solution)/shard_map/all_to_all | solution.py:62
  355.7 1.9 copy.73
  357.6 4.1 all-to-all-start.4
  361.7 0.1 mul.284
  361.9 45.5 %all-to-all-done.4 = bf16[16,2,1,7,2048]{4,1,3,2,0:T(2,128)(2,1)S(1)} async-done(((bf16[16,2,1,7,2048]{4,1,3,2,0:T(2,128)(2,1)}), bf16[16,2,1,7,2048]{4,1,3,2,0:T(2,128)(2,1)S(1)}, u32[]{:S(2)}, u32[]{:S(2)}) %all-to-all-start.4) | async-done | bytes 917536 | tf_op jit(solution)/shard_map/all_to_all | solution.py:62
  407.5 0.4 copy.74
  407.8 0.3 reshape_reshape_reshape.7
  408.1 1.0 gather_fusion
  409.2 0.4 reshape.315
  409.6 0.9 multiply_reduce_fusion
  410.6 0.7 add_convert_fusion
  (62 shorter events, 0.9 us)
Async XLA Ops:
  6.5 1.9 copy-start
  6.6 58.2 %copy-start.11 = (bf16[160,128]{1,0:T(8,128)(2,1)S(1)}, bf16[160,128]{1,0:T(8,128)(2,1)}, u32[]{:S(2)}) copy-start(bf16[160,128]{1,0:T(8,128)(2,1)} %param.16) | copy-start | bytes 122884
  6.6 58.3 %copy-start.10 = (bf16[160,256]{1,0:T(8,128)(2,1)S(1)}, bf16[160,256]{1,0:T(8,128)(2,1)}, u32[]{:S(2)}) copy-start(bf16[160,256]{1,0:T(8,128)(2,1)} %param.15) | copy-start | bytes 245764
  6.6 58.4 %copy-start.13 = (s32[40,4]{0,1:T(4,128)S(1)}, s32[40,4]{0,1:T(4,128)}, u32[]{:S(2)}) copy-start(s32[40,4]{0,1:T(4,128)} %param.28) | copy-start | bytes 1924
  6.6 60.4 %copy-start.12 = (bf16[2048]{0:T(1024)(128)(2,1)S(1)}, bf16[2048]{0:T(1024)(128)(2,1)}, u32[]{:S(2)}) copy-start(bf16[2048]{0:T(1024)(128)(2,1)} %param.24) | copy-start | bytes 12292
  6.6 92.0 %all-gather.2.cloned.1.call-start = ((), (), s32[]{:S(2)}) async-start(), calls=%async_computation.5 | async-start | bytes 5406720 | tf_op jit(solution)/shard_map/all_gather | solution.py:22
  64.7 3.0 copy-start.2
  70.0 28.5 %copy-start.7 = (bf16[160,1,128]{2,1,0:T(2,128)(2,1)S(1)}, bf16[160,1,128]{2,1,0:T(2,128)(2,1)}, u32[]{:S(2)}) copy-start(bf16[160,1,128]{2,1,0:T(2,128)(2,1)} %get-tuple-element.12) | copy-start | bytes 122884
  98.5 3.8 slice-start
  98.5 3.9 slice-start.1
  104.5 11.4 %copy-start.8 = (bf16[40,2048]{1,0:T(8,128)(2,1)S(1)}, bf16[40,2048]{1,0:T(8,128)(2,1)}, u32[]{:S(2)}) copy-start(bf16[40,2048]{1,0:T(8,128)(2,1)} %param.22) | copy-start | bytes 491524
  106.1 9.8 %all-to-all-start = ((bf16[4,40,256]{2,1,0:T(8,128)(2,1)}), bf16[4,40,256]{2,1,0:T(8,128)(2,1)S(1)}, u32[]{:S(2)}, u32[]{:S(2)}) async-start(bf16[4,40,256]{2,1,0:T(8,128)(2,1)} %all_to_all.26), calls=%async_computation | async-start | bytes 163840 | tf_op jit(solution)/shard_map/all_to_all | solution.py:201
  119.0 0.7 copy-start.3
  119.1 10.2 %copy-start.5 = (bf16[1,2048,256]{2,1,0:T(8,128)(2,1)S(1)}, bf16[1,2048,256]{2,1,0:T(8,128)(2,1)}, u32[]{:S(2)}) copy-start(bf16[1,2048,256]{2,1,0:T(8,128)(2,1)} %param.26) | copy-start | bytes 3145732
  120.2 10.5 %copy-start.6 = (bf16[1,2048,256]{2,1,0:T(8,128)(2,1)S(1)}, bf16[1,2048,256]{2,1,0:T(8,128)(2,1)}, u32[]{:S(2)}) copy-start(bf16[1,2048,256]{2,1,0:T(8,128)(2,1)} %param.25) | copy-start | bytes 3145732
  121.5 63.1 %all-to-all-start.1 = ((bf16[32,7,2048]{2,1,0:T(8,128)(2,1)}), bf16[32,7,2048]{2,1,0:T(8,128)(2,1)}, u32[]{:S(2)}, u32[]{:S(2)}) async-start(bf16[32,7,2048]{2,1,0:T(8,128)(2,1)} %reshape.309), calls=%async_computation.1 | async-start | bytes 2097152 | tf_op jit(solution)/shard_map/all_to_all | solution.py:229
  190.7 145.7 %all-to-all-start.2 = ((bf16[4,256,6144]{2,1,0:T(8,128)(2,1)}), bf16[4,256,6144]{2,1,0:T(8,128)(2,1)}, u32[]{:S(2)}, u32[]{:S(2)}) async-start(bf16[4,256,6144]{2,1,0:T(8,128)(2,1)} %stack.25), calls=%async_computation.2 | async-start | bytes 25165824 | tf_op jit(solution)/shard_map/all_to_all | solution.py:33
  350.6 11.1 %copy-start.9 = (s32[40,4]{1,0:T(8,128)S(1)}, s32[40,4]{1,0:T(8,128)}, u32[]{:S(2)}) copy-start(s32[40,4]{1,0:T(8,128)} %get-tuple-element.19) | copy-start | bytes 1924
  350.6 11.2 %copy-start.14 = (f32[40,4]{0,1:T(4,128)S(1)}, f32[40,4]{0,1:T(4,128)}, u32[]{:S(2)}) copy-start(f32[40,4]{0,1:T(4,128)} %param.29) | copy-start | bytes 1924
  357.6 49.9 %all-to-all-start.4 = ((bf16[16,2,1,7,2048]{4,1,3,2,0:T(2,128)(2,1)}), bf16[16,2,1,7,2048]{4,1,3,2,0:T(2,128)(2,1)S(1)}, u32[]{:S(2)}, u32[]{:S(2)}) async-start(bf16[16,2,1,7,2048]{4,1,3,2,0:T(2,128)(2,1)} %copy.73), calls=%async_computation.4 | async-start | bytes 1835008 | tf_op jit(solution)/shard_map/all_to_all | solution.py:62
  408.1 3.1 copy-start.1
  409.2 1.4 copy-start.4
Sparse Core Ops, SparseCore 0:
  11.8 86.7 all-gather.1
